TPU v7x, 32 devices: a whole 2x2x4 slice. The times are simulated.
32 devices in a mesh: ep: 8 (over z, y), tp: 4 (over x, core).
Axes of the slice: x: 2, y: 2, z: 4, core: 2. Of those that a mesh axis runs over, the one named last changes fastest.
Arguments:
- att_queries: bfloat16 [8192, 1024], P(('ep', 'tp')), may hold values from -8 to 8
- att_keys: bfloat16 [8192, 256], P(('ep', 'tp')), may hold values from -6 to 6
- att_values: bfloat16 [8192, 256], P(('ep', 'tp')), may hold values from -6 to 6
- sink_logits: float32 [16], replicated, may hold values from 3 to 6.5
- out_weight: bfloat16 [1024, 2048], replicated, may hold values from -0.1875 to 0.1875
- att_gain: float32 [2048], replicated, may hold values from 0.1 to 1.9
- moe_in: bfloat16 [4096, 2048], P(('ep', 'tp')), may hold values from -6 to 6
- pre_gain: float32 [2048], replicated, may hold values from 0.1 to 1.9
- expert_ids: int32 [4096, 2], P(('ep', 'tp')), may hold values from 0 to 15, all different within a row; in each aligned block of 128 rows (0 to 127, 128 to 255, ...) at most 32 rows name the same one
- routed_expert_weight: float32 [4096, 2], P(('ep', 'tp')), may hold values from 0.2 to 1.5
- w_gate: bfloat16 [16, 2048, 768], P('ep', None, 'tp'), may hold values from -0.125 to 0.125
- w_up: bfloat16 [16, 2048, 768], P('ep', None, 'tp'), may hold values from -0.125 to 0.125
- w_down: bfloat16 [16, 768, 2048], P('ep', 'tp'), may hold values from -0.21875 to 0.21875
- common_expert_gate_weight: bfloat16 [2048, 512], P(None, 'tp'), may hold values from -0.125 to 0.125
- common_expert_up_weight: bfloat16 [2048, 512], P(None, 'tp'), may hold values from -0.125 to 0.125
- common_expert_down_weight: bfloat16 [512, 2048], P('tp'), may hold values from -0.25 to 0.25
- moe_gain: float32 [2048], replicated, may hold values from 0.1 to 1.9
Outputs:
- mixer_out: bfloat16 [8192, 2048], P(('ep', 'tp'))
- experts_out: bfloat16 [4096, 2048], P(('ep', 'tp'))
Inputs may be any that keep to these rules, and one draw needn't show every extreme that they name: `expert_ids`: each row names 2 different experts; within the rows of one device no expert is named more than 32 times, and in every draw some expert is named exactly 32 times by the rows of some device.
All inputs are finite; a program needn't handle non-finite values.
Results may differ from a plain program's by a relative error of at most 0.012.
Values may be sent and summed in bfloat16 or wider, within the bound.
A program may use at most 128 MiB of HBM per device.

v0:
```python
import math
import jax
import jax.numpy as jnp
from jax import lax
from jax.sharding import PartitionSpec as P

HEADS = 16
KV_HEADS = 4
HEAD_DIM = 64
WINDOW = 128
EPS = 1e-06
NEGATIVE = -1e30


def from_behind(block, axis, distance):
    devices = range(lax.axis_size(axis))
    route = [(i - distance, i) for i in devices if i - distance in devices]
    return lax.ppermute(block, axis, route)


def rms_scale(inputs, gain_vec):
    mean_sq = jnp.mean(inputs * inputs, axis=-1, keepdims=True)
    return inputs * lax.rsqrt(mean_sq + EPS) * gain_vec


def slot_table(route_ids, slot_cap):
    flat_ids = route_ids.reshape(-1)
    assigned = flat_ids.shape[0]
    earlier = jnp.arange(assigned)[None, :] < jnp.arange(assigned)[:, None]
    position = jnp.sum((flat_ids[:, None] == flat_ids[None, :]) & earlier, axis=1)
    return (flat_ids * slot_cap + position).reshape(route_ids.shape)


def pack_rows(token_rows, slot_ids, slot_total):
    numbers = jnp.arange(slot_total, dtype=jnp.int32)
    chosen = jnp.any(slot_ids[None, :, :] == numbers[:, None, None], axis=2).astype(jnp.bfloat16)
    return jnp.dot(chosen, token_rows, preferred_element_type=jnp.float32).astype(jnp.bfloat16)


def body(
    att_queries,
    att_keys,
    att_values,
    sink_logits,
    out_weight,
    att_gain,
    moe_in,
    pre_gain,
    expert_ids,
    routed_expert_weight,
    w_gate,
    w_up,
    w_down,
    common_expert_gate_weight,
    common_expert_up_weight,
    common_expert_down_weight,
    moe_gain,
):
    tok_rows = att_queries.shape[0]
    group_size = HEADS // KV_HEADS
    blocks = tok_rows // WINDOW
    kv_rows = jnp.stack([att_keys, att_values])
    rim_rows = from_behind(kv_rows[:, tok_rows - WINDOW :], ("ep", "tp"), 1)
    kv_all = jnp.concatenate([rim_rows, kv_rows], axis=1).reshape(
        2, blocks + 1, WINDOW, KV_HEADS, HEAD_DIM
    )
    kv_band = jnp.concatenate([kv_all[:, :-1], kv_all[:, 1:]], axis=2)
    query_blocks = att_queries.reshape(blocks, WINDOW, KV_HEADS, group_size, HEAD_DIM)
    scores = jnp.einsum(
        "nqgjd,nkgd->ngjqk", query_blocks, kv_band[0], preferred_element_type=jnp.float32
    ) * (1.0 / math.sqrt(HEAD_DIM))
    distance = jnp.arange(WINDOW)[:, None] + WINDOW - jnp.arange(2 * WINDOW)[None, :]
    inside = (distance >= 0) & (distance < WINDOW)
    first_pos = lax.axis_index(("ep", "tp")) * tok_rows
    key_pos = (
        first_pos + jnp.arange(blocks)[:, None] * WINDOW - WINDOW + jnp.arange(2 * WINDOW)[None, :]
    )
    is_valid = inside[None] & (key_pos >= 0)[:, None, :]
    scores = jnp.where(is_valid[:, None, None], scores, NEGATIVE)
    sink_grid = sink_logits.reshape(KV_HEADS, group_size)[None, :, :, None, None]
    row_top = jnp.maximum(jnp.max(scores, axis=-1, keepdims=True), sink_grid)
    exp_scores = jnp.exp(scores - row_top)
    denominator = jnp.sum(exp_scores, axis=-1, keepdims=True) + jnp.exp(sink_grid - row_top)
    probs = (exp_scores / denominator).astype(jnp.bfloat16)
    head_mix = jnp.einsum(
        "ngjqk,nkgd->nqgjd", probs, kv_band[1], preferred_element_type=jnp.float32
    )
    head_mix = head_mix.astype(jnp.bfloat16).reshape(tok_rows, HEADS * HEAD_DIM)
    projected = jnp.dot(head_mix, out_weight, preferred_element_type=jnp.float32)
    mixer_out = rms_scale(projected, att_gain).astype(jnp.bfloat16)
    tokens = moe_in.shape[0]
    top_count = expert_ids.shape[1]
    local_experts = w_gate.shape[0]
    ep_size = lax.axis_size("ep")
    tp_size = lax.axis_size("tp")
    experts = local_experts * ep_size
    slot_cap = 2 * tokens * top_count // experts
    slot_total = experts * slot_cap
    normed = rms_scale(moe_in.astype(jnp.float32), pre_gain).astype(jnp.bfloat16)
    own_slots = slot_table(expert_ids, slot_cap)
    packed = pack_rows(normed, own_slots, slot_total)[None]
    arrived = lax.all_to_all(packed, "ep", split_axis=1, concat_axis=1, tiled=True)
    arrived_all, tokens_all = (
        lax.all_gather(arrived[0], "tp", axis=0, tiled=True),
        lax.all_gather(normed, "tp", axis=0, tiled=True),
    )
    arrived = arrived_all.reshape(tp_size, slot_total, normed.shape[1])
    token_block = tokens_all.reshape(tp_size, tokens, normed.shape[1])
    routed = arrived
    routed = routed.reshape(
        1 * lax.axis_size("tp"), ep_size, local_experts, slot_cap, normed.shape[1]
    )
    gate_act = jnp.einsum("tsjcd,jdf->tsjcf", routed, w_gate, preferred_element_type=jnp.float32)
    up_act = jnp.einsum("tsjcd,jdf->tsjcf", routed, w_up, preferred_element_type=jnp.float32)
    hidden = (jax.nn.silu(gate_act) * up_act).astype(jnp.bfloat16)
    routed_part = jnp.einsum("tsjcf,jfd->tsjcd", hidden, w_down, preferred_element_type=jnp.float32)
    routed_part = routed_part.reshape(1 * lax.axis_size("tp"), slot_total, normed.shape[1])
    common_gate_activation = jnp.einsum(
        "spz,zv->spv", token_block, common_expert_gate_weight, preferred_element_type=jnp.float32
    )
    shared_up_act = jnp.einsum(
        "spz,zv->spv", token_block, common_expert_up_weight, preferred_element_type=jnp.float32
    )
    common_expert_hidden = (jax.nn.silu(common_gate_activation) * shared_up_act).astype(
        jnp.bfloat16
    )
    shared_part = jnp.einsum(
        "nsq,ql->nsl",
        common_expert_hidden,
        common_expert_down_weight,
        preferred_element_type=jnp.float32,
    )
    summed = lax.psum_scatter(
        jnp.concatenate([routed_part, shared_part], axis=1).astype(jnp.bfloat16),
        "tp",
        scatter_dimension=0,
        tiled=True,
    ).astype(jnp.float32)
    routed_out = summed[0, :slot_total].astype(jnp.bfloat16)
    shared_sum = summed[0, slot_total:]
    returned = lax.all_to_all(routed_out, "ep", split_axis=0, concat_axis=0, tiled=True)
    picked = returned[own_slots.reshape(-1)].reshape(tokens, top_count, normed.shape[1])
    combined = (
        jnp.sum(routed_expert_weight[:, :, None] * picked.astype(jnp.float32), axis=1) + shared_sum
    )
    experts_out = rms_scale(combined, moe_gain).astype(jnp.bfloat16)
    return (mixer_out, experts_out)


def solution(mesh):
    in_specs = (
        P(("ep", "tp"), None),
        P(("ep", "tp"), None),
        P(("ep", "tp"), None),
        P(),
        P(),
        P(),
        P(("ep", "tp"), None),
        P(),
        P(("ep", "tp"), None),
        P(("ep", "tp"), None),
        P("ep", None, "tp"),
        P("ep", None, "tp"),
        P("ep", "tp", None),
        P(None, "tp"),
        P(None, "tp"),
        P("tp", None),
        P(),
    )
    out_specs = (P(("ep", "tp"), None), P(("ep", "tp"), None))
    return jax.shard_map(body, mesh=mesh, in_specs=in_specs, out_specs=out_specs, check_vma=False)
```

profile of v0, /device:TPU:0, one launch (start us, length us, event | category | flops | bytes accessed | tf_op | source)
XLA Modules:
  0.0 362.7 jit_solution(12713361354934625359)
XLA Ops:
  11.9 5.2 %copy.111 = bf16[1,512,2048]{2,0,1:T(2,128)(2,1)} copy(bf16[1,512,2048]{2,1,0:T(8,128)(2,1)S(1)} %fusion.6) | data formatting | bytes 4194304 | tf_op jit(solution)/shard_map/broadcast_in_dim | solution.py:101
  17.6 14.5 %reduce = bf16[512,2048]{1,0:T(8,128)(2,1)} reduce(bf16[512,1,2048]{2,1,0:T(2,128)(2,1)} %bitcast.116, bf16[]{:T(256)} %broadcast.169), dimensions={1}, to_apply=%bitcast.113.reduce_sub_computation | reduce | bytes 4194306
  32.1 6.3 %reshape.191 = bf16[8,2,65536]{2,1,0:T(2,128)(2,1)} reshape(bf16[512,2048]{1,0:T(8,128)(2,1)} %reduce) | data formatting | bytes 4194304
  38.4 7.3 %all-to-all-start = ((bf16[8,2,65536]{2,1,0:T(2,128)(2,1)}), bf16[8,2,65536]{2,1,0:T(2,128)(2,1)}, u32[]{:S(2)}, u32[]{:S(2)}) async-start(bf16[8,2,65536]{2,1,0:T(2,128)(2,1)} %reshape.191), calls=%async_computation | async-start | bytes 4194304 | tf_op jit(solution)/shard_map/all_to_all | solution.py:102
  46.5 47.6 %all-to-all-done = bf16[8,2,65536]{2,1,0:T(2,128)(2,1)} async-done(((bf16[8,2,65536]{2,1,0:T(2,128)(2,1)}), bf16[8,2,65536]{2,1,0:T(2,128)(2,1)}, u32[]{:S(2)}, u32[]{:S(2)}) %all-to-all-start) | async-done | bytes 2097184 | tf_op jit(solution)/shard_map/all_to_all | solution.py:102
  94.1 6.8 %reshape.192 = bf16[512,1,2048]{2,1,0:T(2,128)(2,1)} reshape(bf16[8,2,65536]{2,1,0:T(2,128)(2,1)} %all-to-all-done) | data formatting | bytes 4194304
  100.8 4.8 %copy.75 = bf16[1,512,2048]{2,1,0:T(8,128)(2,1)} copy(bf16[1,512,2048]{2,0,1:T(2,128)(2,1)} %bitcast.117) | data formatting | bytes 4194304 | tf_op jit(solution)/shard_map/all_to_all | solution.py:102
  106.6 2.3 fusion.35
  108.9 5.2 %convolution_convert_fusion = bf16[4,128,2048]{2,1,0:T(8,128)(2,1)} fusion(bf16[4,128,2048]{2,1,0:T(8,128)(2,1)} %bitcast.120, bf16[128,2048]{1,0:T(8,128)(2,1)S(1)} %copy-done.8, bf16[2048,128]{1,0:T(8,128)(2,1)S(1)} %copy-done.9, f32[4,128,128]{2,1,0:T(8,128)S(1)} %fusion.35), kind=kOutput, calls=%fused_computation.12 | convolution fusion | flops 538312704 | bytes 5505024 | tf_op jit(solution)/shard_map/nsq,ql->nsl/dot_general | solution.py:127
  114.2 48.9 %all-gather.6.cloned.1.call-done = bf16[1,2048,2048]{2,1,0:T(8,128)(2,1)} async-done(((bf16[1,512,2048]{2,1,0:T(8,128)(2,1)}), bf16[1,2048,2048]{2,1,0:T(8,128)(2,1)}) %all-gather.6.cloned.1.call-update) | async-done | bytes 8388624 | tf_op jit(solution)/shard_map/all_gather | solution.py:104
  163.1 7.6 %fusion.2 = f32[2,4,8,32,192]{4,3,2,1,0:T(8,128)} fusion(bf16[4,8,2,32,2048]{4,3,2,1,0:T(8,128)(2,1)} %bitcast.128, bf16[2,2048,192]{1,2,0:T(8,128)(2,1)} %param.27), kind=kOutput, calls=%fused_computation.5 | convolution fusion | flops 1610612736 | bytes 11534336 | tf_op jit(solution)/shard_map/tsjcd,jdf->tsjcf/dot_general | solution.py:113
  170.7 13.2 %convert_bitcast_fusion = bf16[4,8,2,32,2048]{4,3,1,0,2:T(8,128)(2,1)} fusion(f32[2,4,8,32,192]{4,3,2,1,0:T(8,128)} %fusion.2, bf16[4,8,2,32,2048]{4,3,2,1,0:T(8,128)(2,1)} %bitcast.129, bf16[2,192,2048]{2,1,0:T(8,128)(2,1)S(1)} %copy-done, bf16[2,2048,192]{1,2,0:T(8,128)(2,1)S(1)} %copy-done.15), kind=kOutput, calls=%fused_computation.2 | convolution fusion | flops 3227779072 | bytes 21495808 | tf_op jit(solution)/shard_map/tsjcf,jfd->tsjcd/dot_general | solution.py:116
  183.8 8.4 %copy.78 = bf16[4,8,2,32,2048]{4,3,2,1,0:T(8,128)(2,1)} copy(bf16[4,8,2,32,2048]{4,3,1,0,2:T(8,128)(2,1)} %convert_bitcast_fusion) | data formatting | bytes 16777216 | tf_op jit(solution)/shard_map/tsjcf,jfd->tsjcd/transpose | solution.py:116
  192.3 10.5 %pad_maximum_fusion = bf16[4,640,2048]{2,1,0:T(8,128)(2,1)} fusion(bf16[4,128,2048]{2,1,0:T(8,128)(2,1)S(1)} %copy-done.2, bf16[4,512,2048]{2,1,0:T(8,128)(2,1)} %bitcast.115), kind=kLoop, calls=%fused_computation.1 | loop fusion | flops 20971520 | bytes 20971520 | tf_op jit(solution)/shard_map/concatenate | solution.py:134
  203.7 2.8 collective-permute-start
  206.9 80.4 %reduce-scatter.2.cloned.1.call-done = bf16[1,640,2048]{2,1,0:T(8,128)(2,1)} async-done(((bf16[4,640,2048]{2,1,0:T(8,128)(2,1)}), bf16[1,640,2048]{2,1,0:T(8,128)(2,1)}) %reduce-scatter.2.cloned.1.call-update) | async-done | bytes 2621456 | tf_op jit(solution)/shard_map/reduce_scatter | solution.py:133
  287.3 3.2 slice.36
  290.5 5.6 %all-to-all-start.1 = ((bf16[8,64,2048]{2,1,0:T(8,128)(2,1)}), bf16[8,64,2048]{2,1,0:T(8,128)(2,1)S(1)}, u32[]{:S(2)}, u32[]{:S(2)}) async-start(bf16[8,64,2048]{2,1,0:T(8,128)(2,1)} %bitcast.118), calls=%async_computation.2 | async-start | bytes 4194304 | tf_op jit(solution)/shard_map/all_to_all | solution.py:141
  296.1 1.6 reshape.189
  301.9 2.1 fusion.5
  310.0 34.2 %all-to-all-done.1 = bf16[8,64,2048]{2,1,0:T(8,128)(2,1)S(1)} async-done(((bf16[8,64,2048]{2,1,0:T(8,128)(2,1)}), bf16[8,64,2048]{2,1,0:T(8,128)(2,1)S(1)}, u32[]{:S(2)}, u32[]{:S(2)}) %all-to-all-start.1) | async-done | bytes 2097184 | tf_op jit(solution)/shard_map/all_to_all | solution.py:141
  345.6 2.3 reshape.169
  347.9 4.9 %multiply_reduce_fusion = f32[128,2048]{1,0:T(8,128)S(1)} fusion(f32[128,2,2048]{2,1,0:T(2,128)} %reshape.169, f32[128,2]{1,0:T(8,128)S(1)} %copy.70), kind=kLoop, calls=%fused_computation.22 | loop fusion | flops 786432 | bytes 3146752 | tf_op jit(solution)/shard_map/reduce_sum | solution.py:144
  354.2 2.0 multiply_convert_fusion.1
  (79 shorter events, 21.0 us)
Async XLA Ops:
  7.2 163.5 %copy-start = (bf16[2,192,2048]{2,1,0:T(8,128)(2,1)S(1)}, bf16[2,192,2048]{2,1,0:T(8,128)(2,1)}, u32[]{:S(2)}) copy-start(bf16[2,192,2048]{2,1,0:T(8,128)(2,1)} %param.29) | copy-start | bytes 4718596
  11.2 5.9 %copy-start.3 = (bf16[128,2048]{1,0:T(8,128)(2,1)}, bf16[128,2048]{1,0:T(8,128)(2,1)S(1)}, u32[]{:S(2)}) copy-start(bf16[128,2048]{1,0:T(8,128)(2,1)S(1)} %fusion.25) | copy-start | bytes 1572868
  38.4 55.7 %all-to-all-start = ((bf16[8,2,65536]{2,1,0:T(2,128)(2,1)}), bf16[8,2,65536]{2,1,0:T(2,128)(2,1)}, u32[]{:S(2)}, u32[]{:S(2)}) async-start(bf16[8,2,65536]{2,1,0:T(2,128)(2,1)} %reshape.191), calls=%async_computation | async-start | bytes 4194304 | tf_op jit(solution)/shard_map/all_to_all | solution.py:102
  45.7 60.1 %all-gather.4.cloned.1.call-start = ((), (), s32[]{:S(2)}) async-start(), calls=%async_computation.3 | async-start | bytes 2621440 | tf_op jit(solution)/shard_map/all_gather | solution.py:105
  46.4 116.6 %all-gather.6.cloned.1.call-start = ((), (), s32[]{:S(2)}) async-start(), calls=%async_computation.5 | async-start | bytes 10485760 | tf_op jit(solution)/shard_map/all_gather | solution.py:104
  105.6 1.0 copy-start.7
  105.6 3.3 copy-start.8
  105.6 3.3 copy-start.9
  105.6 181.7 %reduce-scatter.2.cloned.1.call-start = ((), (), s32[]{:S(2)}) async-start(), calls=%async_computation.4 | async-start | bytes 13107200 | tf_op jit(solution)/shard_map/reduce_scatter | solution.py:133
  163.1 7.6 %copy-start.15 = (bf16[2,2048,192]{1,2,0:T(8,128)(2,1)S(1)}, bf16[2,2048,192]{1,2,0:T(8,128)(2,1)}, u32[]{:S(2)}) copy-start(bf16[2,2048,192]{1,2,0:T(8,128)(2,1)} %param.28) | copy-start | bytes 4718596
  183.8 8.4 %copy-start.2 = (bf16[4,128,2048]{2,1,0:T(8,128)(2,1)S(1)}, bf16[4,128,2048]{2,1,0:T(8,128)(2,1)}, u32[]{:S(2)}) copy-start(bf16[4,128,2048]{2,1,0:T(8,128)(2,1)} %convolution_convert_fusion) | copy-start | bytes 6291460
  202.7 0.9 copy-start.5
  202.7 1.0 copy-start.6
  203.7 94.3 %collective-permute-start = (bf16[2,128,256]{2,1,0:T(8,128)(2,1)S(1)}, bf16[2,128,256]{2,1,0:T(8,128)(2,1)}, u32[]{:S(2)}, u32[]{:S(2)}) collective-permute-start(bf16[2,128,256]{2,1,0:T(8,128)(2,1)S(1)} %pad_maximum_fusion.2), channel_id=1, source_target_pairs={{0,1},{1,2},{2,3},{3,4},{4,5},{5,6},{6,7},{7,8},{8,9},{9,10},{10,1... | collective-permute-start | bytes 393224 | tf_op jit(solution)/shard_map/ppermute | solution.py:18
  290.5 5.7 %copy-start.4 = (bf16[256,1024]{1,0:T(8,128)(2,1)S(1)}, bf16[256,1024]{1,0:T(8,128)(2,1)}, u32[]{:S(2)}) copy-start(bf16[256,1024]{1,0:T(8,128)(2,1)} %param.17) | copy-start | bytes 1572868
  290.5 7.3 %copy-start.13 = (f32[16]{0:T(128)S(1)}, f32[16]{0:T(128)}, u32[]{:S(2)}) copy-start(f32[16]{0:T(128)} %param.20) | copy-start | bytes 196
  290.5 7.4 %copy-start.12 = (f32[128,2]{0,1:T(2,128)S(1)}, f32[128,2]{0,1:T(2,128)}, u32[]{:S(2)}) copy-start(f32[128,2]{0,1:T(2,128)} %param.26) | copy-start | bytes 3076
  290.5 53.7 %all-to-all-start.1 = ((bf16[8,64,2048]{2,1,0:T(8,128)(2,1)}), bf16[8,64,2048]{2,1,0:T(8,128)(2,1)S(1)}, u32[]{:S(2)}, u32[]{:S(2)}) async-start(bf16[8,64,2048]{2,1,0:T(8,128)(2,1)} %bitcast.118), calls=%async_computation.2 | async-start | bytes 4194304 | tf_op jit(solution)/shard_map/all_to_all | solution.py:141
  305.2 2.2 copy-start.14
  307.4 1.4 copy-start.10
  347.9 6.2 %copy-start.11 = (f32[2048]{0:T(1024)S(1)}, f32[2048]{0:T(1024)}, u32[]{:S(2)}) copy-start(f32[2048]{0:T(1024)} %param.33) | copy-start | bytes 24580
  347.9 8.3 %copy-start.1 = (bf16[2,192,2048]{2,1,0:T(8,128)(2,1)S(1)}, bf16[2,192,2048]{2,1,0:T(8,128)(2,1)}, u32[]{:S(2)}) copy-start(bf16[2,192,2048]{2,1,0:T(8,128)(2,1)} %param.29) | copy-start | bytes 4718596
Sparse Core Ops, SparseCore 0:
  48.7 23.9 all-gather.3
  105.7 57.2 all-gather.5
  202.9 84.3 reduce-scatter.1
where the time goes:
time: 364 us; the launch traced here: 363 us
  waiting for transfers between devices  212 us (58%)
  local copies, waits for them, and re-layouts  47.7 us (13%)
  other arithmetic  39.5 us (11%)
  matrix products  33.7 us (9%)
  starting transfers between devices  16.1 us (4%)
  between operations  14 us (4%)
    reduce_scatter x1, waiting for transfers between devices, body(): lax.psum_scatter(jnp.concatenate([routed_part, shared_part], axis=1).asty...  80.4 us
    all_gather x1, waiting for transfers between devices, body(): lax.all_gather(arrived[0], 'tp', axis=0, tiled=True)  48.9 us
    all_to_all x1, waiting for transfers between devices, body(): lax.all_to_all(packed, 'ep', split_axis=1, concat_axis=1, tiled=True)  47.6 us
    all_to_all x1, waiting for transfers between devices, body(): lax.all_to_all(routed_out, 'ep', split_axis=0, concat_axis=0, tiled=True)  34.2 us
    unnamed x39, local copies, waits for them, and re-layouts  18.3 us
    unnamed x1, other arithmetic  14.5 us
    dot_general x1, matrix products, body(): jnp.einsum('tsjcf,jfd->tsjcd', hidden, w_down, preferred_element_type=jnp...  13.2 us
    concatenate x1, other arithmetic, body(): jnp.concatenate([routed_part, shared_part], axis=1).astype(jnp.bfloat16)  10.5 us
  transfers between devices with their start and end apart: 6, of which 4 were waited for; matrix products, arithmetic and copies ran while one was open for 10% of the time, Pallas kernels for 0%

commit v1 on v0

--- a/solution.py
+++ b/solution.py
@@ -99,7 +99,10 @@
     normed = rms_scale(moe_in.astype(jnp.float32), pre_gain).astype(jnp.bfloat16)
     own_slots = slot_table(expert_ids, slot_cap)
     packed = pack_rows(normed, own_slots, slot_total)[None]
-    arrived = lax.all_to_all(packed, "ep", split_axis=1, concat_axis=1, tiled=True)
+    arrived = jnp.concatenate(
+        lax.all_to_all(jnp.stack(jnp.split(packed, lax.axis_size("ep"), axis=1)), "ep", 0, 0),
+        axis=1,
+    )
     arrived_all, tokens_all = (
         lax.all_gather(arrived[0], "tp", axis=0, tiled=True),
         lax.all_gather(normed, "tp", axis=0, tiled=True),

time: 364 us -> 331 us (0.909)
  local copies, waits for them, and re-layouts: 47.7 us -> 29.2 us
  other arithmetic: 39.5 us -> 25 us
    unnamed x1 -> x0, other arithmetic: 14.5 us -> none
    unnamed x39 -> x43, local copies, waits for them, and re-layouts: 18.3 us -> 8.98 us
    broadcast_in_dim x1 -> x0, local copies, waits for them, and re-layouts: 5.17 us -> none  [body(): packed = pack_rows(normed, own_slots, slot_total)[None]]
    all_to_all x1 -> x0, local copies, waits for them, and re-layouts: 4.77 us -> none  [body(): lax.all_to_all(packed, 'ep', split_axis=1, concat_axis=1, tiled=True)]
  transfers between devices with their start and end apart: 6 -> 6, of which waited for: 4 -> 4; matrix products, arithmetic and copies ran while one was open for 10% -> 7% of each run, Pallas kernels for 0% -> 0%
where the time goes in v1:
time: 331 us
  waiting for transfers between devices  213 us (64%)
  matrix products  33.8 us (10%)
  local copies, waits for them, and re-layouts  29.2 us (9%)
  other arithmetic  25 us (8%)
  starting transfers between devices  15.9 us (5%)
  between operations  14 us (4%)
    reduce_scatter x1, waiting for transfers between devices, body(): lax.psum_scatter(jnp.concatenate([routed_part, shared_part], axis=1).asty...  80.4 us
    all_gather x1, waiting for transfers between devices, body(): lax.all_gather(arrived[0], 'tp', axis=0, tiled=True)  49.7 us
    all_to_all x1, waiting for transfers between devices, body(): lax.all_to_all(jnp.stack(jnp.split(packed, lax.axis_size('ep'), axis=1)),...  47.6 us
    all_to_all x1, waiting for transfers between devices, body(): lax.all_to_all(routed_out, 'ep', split_axis=0, concat_axis=0, tiled=True)  34.2 us
    dot_general x1, matrix products, body(): jnp.einsum('tsjcf,jfd->tsjcd', hidden, w_down, preferred_element_type=jnp...  13.2 us
    concatenate x1, other arithmetic, body(): jnp.concatenate([routed_part, shared_part], axis=1).astype(jnp.bfloat16)  10.4 us
    unnamed x43, local copies, waits for them, and re-layouts  8.98 us
    transpose x1, local copies, waits for them, and re-layouts, body(): jnp.einsum('tsjcf,jfd->tsjcd', hidden, w_down, preferred_element_type=jnp...  8.43 us
  transfers between devices with their start and end apart: 6, of which 4 were waited for; matrix products, arithmetic and copies ran while one was open for 7% of the time, Pallas kernels for 0%

profile of v1, /device:TPU:0, one launch (start us, length us, event | category | flops | bytes accessed | tf_op | source)
XLA Modules:
  0.0 330.5 jit_solution(4239750972461434371)
XLA Ops:
  10.0 1.2 fusion.25
  17.6 7.3 %all-to-all-start = ((bf16[8,1,64,2048]{3,2,1,0:T(8,128)(2,1)}), bf16[8,1,64,2048]{3,2,1,0:T(8,128)(2,1)}, u32[]{:S(2)}, u32[]{:S(2)}) async-start(bf16[8,1,64,2048]{3,2,1,0:T(8,128)(2,1)} %fusion.41), calls=%async_computation | async-start | bytes 4194304 | tf_op jit(solution)/shard_map/all_to_all | solution.py:103
  25.7 47.6 %all-to-all-done = bf16[8,1,64,2048]{3,2,1,0:T(8,128)(2,1)} async-done(((bf16[8,1,64,2048]{3,2,1,0:T(8,128)(2,1)}), bf16[8,1,64,2048]{3,2,1,0:T(8,128)(2,1)}, u32[]{:S(2)}, u32[]{:S(2)}) %all-to-all-start) | async-done | bytes 2097184 | tf_op jit(solution)/shard_map/all_to_all | solution.py:103
  73.4 2.4 fusion.35
  75.8 5.3 %convolution_convert_fusion = bf16[4,128,2048]{2,1,0:T(8,128)(2,1)} fusion(bf16[4,128,2048]{2,1,0:T(8,128)(2,1)} %bitcast.147, bf16[128,2048]{1,0:T(8,128)(2,1)S(1)} %copy-done.8, bf16[2048,128]{1,0:T(8,128)(2,1)S(1)} %copy-done.9, f32[4,128,128]{2,1,0:T(8,128)S(1)} %fusion.35), kind=kOutput, calls=%fused_computation.12 | convolution fusion | flops 538312704 | bytes 5505024 | tf_op jit(solution)/shard_map/nsq,ql->nsl/dot_general | solution.py:130
  81.1 49.7 %all-gather.3.cloned.1.call-done = bf16[2048,2048]{1,0:T(8,128)(2,1)} async-done(((bf16[512,2048]{1,0:T(8,128)(2,1)}), bf16[2048,2048]{1,0:T(8,128)(2,1)}) %all-gather.3.cloned.1.call-update) | async-done | bytes 8388624 | tf_op jit(solution)/shard_map/all_gather | solution.py:107
  130.8 7.6 %fusion.2 = f32[2,4,8,32,192]{4,3,2,1,0:T(8,128)} fusion(bf16[4,8,2,32,2048]{4,3,2,1,0:T(8,128)(2,1)} %bitcast.155, bf16[2,2048,192]{1,2,0:T(8,128)(2,1)} %param.27), kind=kOutput, calls=%fused_computation.5 | convolution fusion | flops 1610612736 | bytes 11534336 | tf_op jit(solution)/shard_map/tsjcd,jdf->tsjcf/dot_general | solution.py:116
  138.4 13.2 %convert_bitcast_fusion = bf16[4,8,2,32,2048]{4,3,1,0,2:T(8,128)(2,1)} fusion(f32[2,4,8,32,192]{4,3,2,1,0:T(8,128)} %fusion.2, bf16[4,8,2,32,2048]{4,3,2,1,0:T(8,128)(2,1)} %bitcast.156, bf16[2,192,2048]{2,1,0:T(8,128)(2,1)S(1)} %copy-done, bf16[2,2048,192]{1,2,0:T(8,128)(2,1)S(1)} %copy-done.15), kind=kOutput, calls=%fused_computation.2 | convolution fusion | flops 3227779072 | bytes 21495808 | tf_op jit(solution)/shard_map/tsjcf,jfd->tsjcd/dot_general | solution.py:119
  151.6 8.4 %copy.48 = bf16[4,8,2,32,2048]{4,3,2,1,0:T(8,128)(2,1)} copy(bf16[4,8,2,32,2048]{4,3,1,0,2:T(8,128)(2,1)} %convert_bitcast_fusion) | data formatting | bytes 16777216 | tf_op jit(solution)/shard_map/tsjcf,jfd->tsjcd/transpose | solution.py:119
  160.0 10.4 %pad_maximum_fusion = bf16[4,640,2048]{2,1,0:T(8,128)(2,1)} fusion(bf16[4,128,2048]{2,1,0:T(8,128)(2,1)S(1)} %copy-done.2, bf16[4,512,2048]{2,1,0:T(8,128)(2,1)} %bitcast.144), kind=kLoop, calls=%fused_computation.1 | loop fusion | flops 20971520 | bytes 20971520 | tf_op jit(solution)/shard_map/concatenate | solution.py:137
  171.4 2.8 collective-permute-start
  174.7 80.4 %reduce-scatter.2.cloned.1.call-done = bf16[1,640,2048]{2,1,0:T(8,128)(2,1)} async-done(((bf16[4,640,2048]{2,1,0:T(8,128)(2,1)}), bf16[1,640,2048]{2,1,0:T(8,128)(2,1)}) %reduce-scatter.2.cloned.1.call-update) | async-done | bytes 2621456 | tf_op jit(solution)/shard_map/reduce_scatter | solution.py:136
  255.0 3.2 slice.36
  258.2 5.7 %all-to-all-start.1 = ((bf16[8,64,2048]{2,1,0:T(8,128)(2,1)}), bf16[8,64,2048]{2,1,0:T(8,128)(2,1)S(1)}, u32[]{:S(2)}, u32[]{:S(2)}) async-start(bf16[8,64,2048]{2,1,0:T(8,128)(2,1)} %bitcast.145), calls=%async_computation.2 | async-start | bytes 4194304 | tf_op jit(solution)/shard_map/all_to_all | solution.py:144
  264.0 1.6 reshape.187
  268.2 1.3 copy.59
  269.7 2.1 fusion.5
  275.2 1.4 multiply_reduce_fusion.1
  277.8 34.2 %all-to-all-done.1 = bf16[8,64,2048]{2,1,0:T(8,128)(2,1)S(1)} async-done(((bf16[8,64,2048]{2,1,0:T(8,128)(2,1)}), bf16[8,64,2048]{2,1,0:T(8,128)(2,1)S(1)}, u32[]{:S(2)}, u32[]{:S(2)}) %all-to-all-start.1) | async-done | bytes 2097184 | tf_op jit(solution)/shard_map/all_to_all | solution.py:144
  312.0 1.4 gather_fusion
  313.3 2.4 reshape.169
  315.7 4.9 %multiply_reduce_fusion = f32[128,2048]{1,0:T(8,128)S(1)} fusion(f32[128,2,2048]{2,1,0:T(2,128)} %reshape.169, f32[128,2]{1,0:T(8,128)S(1)} %copy.42), kind=kLoop, calls=%fused_computation.22 | loop fusion | flops 786432 | bytes 3146752 | tf_op jit(solution)/shard_map/reduce_sum | solution.py:147
  320.6 1.3 multiply_reduce_fusion.2
  321.9 2.0 multiply_convert_fusion.1
  (81 shorter events, 18.8 us)
Async XLA Ops:
  7.2 131.2 %copy-start = (bf16[2,192,2048]{2,1,0:T(8,128)(2,1)S(1)}, bf16[2,192,2048]{2,1,0:T(8,128)(2,1)}, u32[]{:S(2)}) copy-start(bf16[2,192,2048]{2,1,0:T(8,128)(2,1)} %param.29) | copy-start | bytes 4718596
  11.2 2.9 copy-start.3
  17.6 55.7 %all-to-all-start = ((bf16[8,1,64,2048]{3,2,1,0:T(8,128)(2,1)}), bf16[8,1,64,2048]{3,2,1,0:T(8,128)(2,1)}, u32[]{:S(2)}, u32[]{:S(2)}) async-start(bf16[8,1,64,2048]{3,2,1,0:T(8,128)(2,1)} %fusion.41), calls=%async_computation | async-start | bytes 4194304 | tf_op jit(solution)/shard_map/all_to_all | solution.py:103
  25.0 48.4 %copy-start.7 = (bf16[2048,128]{1,0:T(8,128)(2,1)S(1)}, bf16[2048,128]{1,0:T(8,128)(2,1)}, u32[]{:S(2)}) copy-start(bf16[2048,128]{1,0:T(8,128)(2,1)} %param.30) | copy-start | bytes 1572868
  25.0 48.4 %all-gather.5.cloned.1.call-start = ((), (), s32[]{:S(2)}) async-start(), calls=%async_computation.4 | async-start | bytes 2621440 | tf_op jit(solution)/shard_map/all_gather | solution.py:108
  25.7 105.1 %all-gather.3.cloned.1.call-start = ((), (), s32[]{:S(2)}) async-start(), calls=%async_computation.3 | async-start | bytes 10485760 | tf_op jit(solution)/shard_map/all_gather | solution.py:107
  73.3 2.5 copy-start.8
  73.3 2.5 copy-start.9
  73.3 181.7 %reduce-scatter.2.cloned.1.call-start = ((), (), s32[]{:S(2)}) async-start(), calls=%async_computation.5 | async-start | bytes 13107200 | tf_op jit(solution)/shard_map/reduce_scatter | solution.py:136
  130.8 7.6 %copy-start.15 = (bf16[2,2048,192]{1,2,0:T(8,128)(2,1)S(1)}, bf16[2,2048,192]{1,2,0:T(8,128)(2,1)}, u32[]{:S(2)}) copy-start(bf16[2,2048,192]{1,2,0:T(8,128)(2,1)} %param.28) | copy-start | bytes 4718596
  151.6 8.4 %copy-start.2 = (bf16[4,128,2048]{2,1,0:T(8,128)(2,1)S(1)}, bf16[4,128,2048]{2,1,0:T(8,128)(2,1)}, u32[]{:S(2)}) copy-start(bf16[4,128,2048]{2,1,0:T(8,128)(2,1)} %convolution_convert_fusion) | copy-start | bytes 6291460
  170.5 0.9 copy-start.5
  170.5 1.0 copy-start.6
  171.4 94.3 %collective-permute-start = (bf16[2,128,256]{2,1,0:T(8,128)(2,1)S(1)}, bf16[2,128,256]{2,1,0:T(8,128)(2,1)}, u32[]{:S(2)}, u32[]{:S(2)}) collective-permute-start(bf16[2,128,256]{2,1,0:T(8,128)(2,1)S(1)} %pad_maximum_fusion.2), channel_id=1, source_target_pairs={{0,1},{1,2},{2,3},{3,4},{4,5},{5,6},{6,7},{7,8},{8,9},{9,10},{10,1... | collective-permute-start | bytes 393224 | tf_op jit(solution)/shard_map/ppermute | solution.py:18
  258.2 5.7 %copy-start.12 = (f32[128,2]{0,1:T(2,128)S(1)}, f32[128,2]{0,1:T(2,128)}, u32[]{:S(2)}) copy-start(f32[128,2]{0,1:T(2,128)} %param.26) | copy-start | bytes 3076
  258.2 5.8 %copy-start.4 = (bf16[256,1024]{1,0:T(8,128)(2,1)S(1)}, bf16[256,1024]{1,0:T(8,128)(2,1)}, u32[]{:S(2)}) copy-start(bf16[256,1024]{1,0:T(8,128)(2,1)} %param.17) | copy-start | bytes 1572868
  258.2 7.4 %copy-start.13 = (f32[16]{0:T(128)S(1)}, f32[16]{0:T(128)}, u32[]{:S(2)}) copy-start(f32[16]{0:T(128)} %param.20) | copy-start | bytes 196
  258.2 53.7 %all-to-all-start.1 = ((bf16[8,64,2048]{2,1,0:T(8,128)(2,1)}), bf16[8,64,2048]{2,1,0:T(8,128)(2,1)S(1)}, u32[]{:S(2)}, u32[]{:S(2)}) async-start(bf16[8,64,2048]{2,1,0:T(8,128)(2,1)} %bitcast.145), calls=%async_computation.2 | async-start | bytes 4194304 | tf_op jit(solution)/shard_map/all_to_all | solution.py:144
  273.0 2.2 copy-start.14
  275.2 1.4 copy-start.10
  315.7 6.2 %copy-start.11 = (f32[2048]{0:T(1024)S(1)}, f32[2048]{0:T(1024)}, u32[]{:S(2)}) copy-start(f32[2048]{0:T(1024)} %param.33) | copy-start | bytes 24580
  315.7 8.3 %copy-start.1 = (bf16[2,192,2048]{2,1,0:T(8,128)(2,1)S(1)}, bf16[2,192,2048]{2,1,0:T(8,128)(2,1)}, u32[]{:S(2)}) copy-start(bf16[2,192,2048]{2,1,0:T(8,128)(2,1)} %param.29) | copy-start | bytes 4718596
Sparse Core Ops, SparseCore 0:
  27.9 23.9 all-gather.4
  73.4 57.2 all-gather.2
  170.6 84.3 reduce-scatter.1
